TPU v7x, 32 devices: a whole 2x2x4 slice. The times are simulated.
32 devices in a mesh: fs: 8 (over z, y), tp: 4 (over x, core).
Axes of the slice: x: 2, y: 2, z: 4, core: 2. Of those that a mesh axis runs over, the one named last changes fastest.
Arguments:
- tokens: bfloat16 [4096, 2048], P(('fs', 'tp')), may hold values from -6 to 6
- pre_gain: float32 [2048], replicated, may hold values from 0.1 to 1.9
- w_expand: bfloat16 [2048, 8192], P('fs', 'tp'), may hold values from -0.125 to 0.125
- w_reduce: bfloat16 [8192, 2048], P('tp', 'fs'), may hold values from -0.0625 to 0.0625
- post_gain: float32 [2048], replicated, may hold values from 0.1 to 1.9
Outputs:
- result: bfloat16 [4096, 2048], P(('fs', 'tp'))
All inputs are finite; a program needn't handle non-finite values.
Results may differ from a plain program's by a relative error of at most 0.014.
Values may be sent and summed in bfloat16 or wider, within the bound.
A program may use at most 64 MiB of HBM per device.

v0:
```python
import functools

import jax
import jax.numpy as jnp
from jax import lax
from jax.experimental import pallas as pl
from jax.experimental.pallas import tpu as pltpu
from jax.sharding import PartitionSpec as P

NORM_EPS = 1e-06
MESH = pl.DeviceIdType.MESH


def kernel(NX, NY, NZ, tok, gain_in, w_e, w_r, gain_out, out,
           TG, N, WE, WR, H, O, PR, RX,
           t_ls, t_ps, t_r, e_a, e_b, e_c, e_l, e_r, r_a, r_b, r_c, r_l, r_r, p_s, p_r, c_s, c_r):
    R, D = tok.shape
    DK, F = w_e.shape
    H4 = F // NZ
    fs, tp = lax.axis_index("fs"), lax.axis_index("tp")
    z, y = fs // NY, fs % NY
    x, c = tp // 2, tp % 2
    pc = 1 - c
    peer = (fs, x * 2 + pc)

    def zdev(q):
        return (q * NY + y, tp)

    xs = [(x + j) % NX for j in range(1, NX)]
    ys = [(y + j) % NY for j in range(1, NY)]
    xdevs = [(fs, q * 2 + c) for q in xs]
    ydevs = [(z * NY + q, tp) for q in ys]

    barrier = pltpu.get_barrier_semaphore()
    others = [zdev((z + j) % NZ) for j in range(1, NZ)] + xdevs + ydevs + [peer]
    for dev in others:
        pl.semaphore_signal(barrier, inc=1, device_id=dev, device_id_type=MESH)
    pl.semaphore_wait(barrier, len(others))

    def rc(src, dst, ss, rs, dev):
        return pltpu.make_async_remote_copy(src_ref=src, dst_ref=dst, send_sem=ss, recv_sem=rs,
                                            device_id=dev, device_id_type=MESH)

    sent = []

    def go(cond, make):
        if cond is None:
            make().start()
        else:
            pl.when(cond)(lambda: make().start())
        sent.append((cond, make))

    def guarded(cond, fn):
        if cond is None:
            fn()
        else:
            pl.when(cond)(fn)

    def at_distance(d):
        if d == 0:
            return [(z, 0, None)]
        return [(z - d, -1, z - d >= 0), (z + d, 1, z + d < NZ)]

    def rows_of(start, size, half):
        if half is None:
            return pl.ds(pl.multiple_of(start, size), size)
        return pl.ds(pl.multiple_of(start + half * (size // 2), size // 2), size // 2)

    def e_view(xq, zq, yq, half=None):
        return WE.at[xq, rows_of((zq * NY + yq) * DK, DK, half)]

    def r_view(xq, zq, yq, half=None):
        return WR.at[zq * NY + yq, rows_of(xq * H4, H4, half)]

    def e_piece(q):
        return w_e.at[:, pl.ds(pl.multiple_of(q * H4, H4), H4)]

    def r_piece(q):
        return w_r.at[pl.ds(pl.multiple_of(q * H4, H4), H4)]

    own = [
        pltpu.make_async_copy(tok, TG.at[z, c], t_r.at[z, c]),
        pltpu.make_async_copy(e_piece(z), e_view(x, z, y), e_l.at[z]),
        pltpu.make_async_copy(r_piece(z), r_view(x, z, y), r_l.at[z]),
    ]
    for copy in own:
        copy.start()
    def line_pieces(view, piece, a_s, r):
        for d in range(1, NZ):
            for q, s, ok in at_distance(d):
                go(ok, lambda q=q: rc(piece(q), view(x, z, y), a_s.at[q], r.at[z], zdev(q)))

    def own_tokens():
        for side, (q, ok) in enumerate(((z - 1, z >= 1), (z + 1, z + 1 < NZ))):
            go(ok, lambda q=q, side=side: rc(tok, TG.at[z, c], t_ls.at[z, side], t_r.at[z, c], zdev(q)))
        go(None, lambda: rc(tok, TG.at[z, c], t_ps.at[z], t_r.at[z, c], peer))

    line_pieces(e_view, e_piece, e_a, e_l)
    own_tokens()
    line_pieces(r_view, r_piece, r_a, r_l)

    def landed(ref, sem):
        pltpu.make_async_copy(ref, ref, sem).wait()

    def tokens_step(d):
        for q, s, ok in at_distance(d):
            guarded(ok, lambda q=q: landed(TG.at[q, c], t_r.at[q, c]))
            if d > 0:
                n = z - s
                go(jnp.logical_and(ok, jnp.logical_and(n >= 0, n < NZ)),
                   lambda q=q, n=n, s=s: rc(TG.at[q, c], TG.at[q, c], t_ls.at[q, (1 - s) // 2],
                                            t_r.at[q, c], zdev(n)))
                go(ok, lambda q=q: rc(TG.at[q, c], TG.at[q, c], t_ps.at[q], t_r.at[q, c], peer))

    ways = ((xdevs, xs, ydevs, ys), (ydevs, ys, xdevs, xs))

    def first_step(d, view, l, r, b_s, c_s_):
        for q, s, ok in at_distance(d):
            guarded(ok, lambda q=q: landed(view(x, q, y), l.at[q]))
            for h in (0, 1):
                for j, dev in enumerate(ways[h][0]):
                    go(ok, lambda q=q, j=j, dev=dev, h=h: rc(view(x, q, y, h), view(x, q, y, h), b_s.at[q, j, h],
                                                             r.at[x, q, y, h], dev))
            for h in (0, 1):
                for j, dev in enumerate(ways[h][2]):
                    go(ok, lambda q=q, j=j, dev=dev, h=h: rc(view(x, q, y, h), view(x, q, y, h), c_s_.at[q, 0, j, h],
                                                             r.at[x, q, y, h], dev))

    def second_step(d, view, r, c_s_):
        for q, s, ok in at_distance(d):
            for h in (0, 1):
                for i, m in enumerate(ways[h][1]):
                    where = (m, q, y) if h == 0 else (x, q, m)
                    guarded(ok, lambda where=where, h=h: landed(view(*where, h), r.at[(*where, h)]))
                    for j, dev in enumerate(ways[h][2]):
                        go(ok, lambda q=q, i=i, j=j, dev=dev, where=where, h=h:
                           rc(view(*where, h), view(*where, h), c_s_.at[q, 1 + i, j, h], r.at[(*where, h)], dev))

    def last_step(d, view, r):
        for q, s, ok in at_distance(d):
            for h in (0, 1):
                for a in [x] + xs if h == 0 else xs:
                    for b in ys if h == 0 else [y] + ys:
                        guarded(ok, lambda a=a, b=b, q=q, h=h: landed(view(a, q, b, h), r.at[a, q, b, h]))

    M = 2 * R
    sub = 32

    def expand_rows(q):
        landed(TG.at[q, pc], t_r.at[q, pc])

        def norm(i, carry):
            v = TG[q, i // (R // sub), pl.ds(pl.multiple_of((i % (R // sub)) * sub, sub), sub)].astype(jnp.float32)
            v = v * lax.rsqrt(jnp.mean(v * v, axis=-1, keepdims=True) + NORM_EPS) * gain_in[...]
            N[pl.ds(pl.multiple_of(i * sub, sub), sub)] = v.astype(jnp.bfloat16)
            return carry

        lax.fori_loop(0, M // sub, norm, 0)

        def expand(i, carry):
            p = jnp.dot(N[...], WE[i], preferred_element_type=jnp.float32)
            H[i, pl.ds(pl.multiple_of(q * M, M), M)] = jnp.square(jnp.maximum(p, 0.0)).astype(jnp.bfloat16)
            return carry

        lax.fori_loop(0, NX, expand, 0)

    big = 2 * M if NZ % 2 == 0 else M

    def columns(q):
        def body(k, carry):
            f, i = q * NY + k // (NZ * M // big), k % (NZ * M // big)
            row = pl.ds(pl.multiple_of(i * big, big), big)
            p = jnp.dot(H[0, row], WR[f, :H4], preferred_element_type=jnp.float32)
            for xq in range(1, NX):
                p += jnp.dot(H[xq, row], WR[f, xq * H4:(xq + 1) * H4], preferred_element_type=jnp.float32)
            O[pl.ds(i * (big // R), big // R), f] = p.astype(jnp.bfloat16).reshape(big // R, R, DK)
            return carry

        lax.fori_loop(0, NY * NZ * M // big, body, 0)

    tokens_step(0)
    for d in range(NZ):
        first_step(d, e_view, e_l, e_r, e_b, e_c)
        if d == 0:
            first_step(d, r_view, r_l, r_r, r_b, r_c)
        if d > 0:
            second_step(d - 1, e_view, e_r, e_c)
        if d == NZ - 1:
            tokens_step(1)
    second_step(NZ - 1, e_view, e_r, e_c)
    second_step(0, r_view, r_r, r_c)
    for d in range(1, NZ):
        first_step(d, r_view, r_l, r_r, r_b, r_c)
        if d > 1:
            second_step(d - 1, r_view, r_r, r_c)
            tokens_step(d)
    for d in range(NZ):
        last_step(d, e_view, e_r)

    def expand_at(d):
        for q, s, ok in at_distance(d):
            guarded(ok, lambda q=q: expand_rows(q))

    expand_at(0)
    expand_at(1)
    second_step(NZ - 1, r_view, r_r, r_c)
    for d in range(2, NZ):
        expand_at(d)
    for d in range(NZ):
        last_step(d, r_view, r_r)
        for q, s, ok in at_distance(d):
            guarded(ok, lambda q=q: columns(q))

    FH = NZ * NY // 2

    def part(h):
        return pl.ds(h * FH, FH)

    order = []
    for k in range((NZ + 1) // 2):
        order += [NZ - 1 - k] + ([k] if k != NZ - 1 - k else [])
    for h in (0, 1):
        for q in order:
            go(None, lambda q=q, h=h: rc(O.at[q * 2 + pc, part(h)], PR.at[q, part(h)], p_s.at[q, h], p_r.at[q, h], peer))

    def add_part(q, h, slots):
        landed(PR.at[q, part(h)], p_r.at[q, h])
        for slot in slots:
            landed(RX.at[slot, part(h)], c_r.at[slot, h])

        def body(f, carry):
            s = O[q * 2 + c, f].astype(jnp.float32) + PR[q, f].astype(jnp.float32)
            for slot in slots:
                s += RX[slot, f].astype(jnp.float32)
            O[q * 2 + c, f] = s.astype(jnp.bfloat16)
            return carry

        lax.fori_loop(h * FH, (h + 1) * FH, body, 0)

    for j in range(NZ - 1):
        for h in (0, 1):
            for q, n, ok, has in ((NZ - 1 - j, z + 1, NZ - 1 - j > z, z > 0), (j, z - 1, j < z, z < NZ - 1)):
                pl.when(jnp.logical_and(ok, has))(lambda q=q, h=h: add_part(q, h, [q]))
                pl.when(jnp.logical_and(ok, jnp.logical_not(has)))(lambda q=q, h=h: add_part(q, h, []))
                slot = jnp.where(jnp.logical_and(n < z, n == q), NZ, q)
                go(ok, lambda q=q, n=n, slot=slot, h=h: rc(O.at[q * 2 + c, part(h)], RX.at[slot, part(h)],
                                                           c_s.at[q, h], c_r.at[slot, h], zdev(n)))
    for h in (0, 1):
        pl.when(jnp.logical_and(z > 0, z < NZ - 1))(lambda h=h: add_part(z, h, [z, NZ]))
        pl.when(z == 0)(lambda h=h: add_part(z, h, [NZ]))
        pl.when(z == NZ - 1)(lambda h=h: add_part(z, h, [z]))

    def squares(f, acc):
        m = O[z * 2 + c, f].astype(jnp.float32)
        return acc + jnp.sum(m * m, axis=-1, keepdims=True)

    total = lax.fori_loop(0, NZ * NY, squares, jnp.zeros((R, 1), jnp.float32))
    scale = lax.rsqrt(total / D + NORM_EPS)
    for f in range(NZ * NY):
        cols = slice(f * DK, (f + 1) * DK)
        out[:, cols] = (O[z * 2 + c, f].astype(jnp.float32) * scale * gain_out[:, cols]).astype(jnp.bfloat16)

    for cond, make in sent:
        guarded(cond, lambda make=make: make().wait_send())


def per_device(FS, TP, tokens, pre_gain, w_expand, w_reduce, post_gain):
    NX = TP // 2
    NY = max(k for k in range(1, FS + 1) if FS % k == 0 and (k == 1 or 2 * k * k <= FS))
    NZ = FS // NY
    R, D = tokens.shape
    DK, F = w_expand.shape
    H4 = F // NZ
    bf = jnp.bfloat16
    dma = pltpu.SemaphoreType.DMA
    mx = max(NX, NY)
    vmem = pl.BlockSpec(memory_space=pltpu.VMEM)
    hbm = pl.BlockSpec(memory_space=pl.ANY)
    return pl.pallas_call(
        functools.partial(kernel, NX, NY, NZ),
        out_shape=jax.ShapeDtypeStruct((R, D), bf),
        in_specs=[hbm, vmem, hbm, hbm, vmem],
        out_specs=vmem,
        scratch_shapes=[
            pltpu.VMEM((NZ, 2, R, D), bf),
            pltpu.VMEM((2 * R, D), bf),
            pltpu.VMEM((NX, D, H4), bf),
            pltpu.VMEM((FS, NX * H4, DK), bf),
            pltpu.VMEM((NX, NZ * 2 * R, H4), bf),
            pltpu.VMEM((NZ * 2, FS, R, DK), bf),
            pltpu.VMEM((NZ, FS, R, DK), bf),
            pltpu.VMEM((NZ + 1, FS, R, DK), bf),
            dma((NZ, 2)), dma((NZ,)), dma((NZ, 2)),
            dma((NZ,)), dma((NZ, mx, 2)), dma((NZ, mx, mx, 2)), dma((NZ,)), dma((NX, NZ, NY, 2)),
            dma((NZ,)), dma((NZ, mx, 2)), dma((NZ, mx, mx, 2)), dma((NZ,)), dma((NX, NZ, NY, 2)),
            dma((NZ, 2)), dma((NZ, 2)), dma((NZ, 2)), dma((NZ + 1, 2)),
        ],
        compiler_params=pltpu.CompilerParams(
            collective_id=0, has_side_effects=True, vmem_limit_bytes=64 * 1024 * 1024 - 128 * 1024),
    )(tokens, pre_gain.reshape(1, D), w_expand, w_reduce, post_gain.reshape(1, D))


def solution(mesh):
    return jax.shard_map(
        functools.partial(per_device, mesh.shape["fs"], mesh.shape["tp"]),
        mesh=mesh,
        in_specs=(P(("fs", "tp"), None), P(), P("fs", "tp"), P("tp", "fs"), P()),
        out_specs=P(("fs", "tp"), None),
        check_vma=False,
    )
```

profile of v0, /device:TPU:20, one launch (start us, length us, event | category | flops | bytes accessed | tf_op | source)
XLA Modules:
  0.0 158.3 jit_solution(6799990072475000852)
XLA Ops:
  0.0 156.4 %shard_map.55 = bf16[128,2048]{1,0:T(8,128)(2,1)} custom-call(bf16[128,2048]{1,0:T(8,128)(2,1)} %tok.1, f32[1,2048]{1,0:T(1,128)} %bitcast.2, bf16[256,2048]{1,0:T(8,128)(2,1)} %w_e.1, bf16[2048,256]{1,0:T(8,128)(2,1)} %w_r.1, f32[1,2048]{1,0:T(1,128)} %bitcast.3), custom_call_target="tpu_custom_call" | custom-call | tf_op jit(solution)/shard_map/pallas_call | solution.py:279
  156.4 1.9 %copy.7 = bf16[128,2048]{1,0:T(8,128)(2,1)} copy(bf16[128,2048]{1,0:T(8,128)(2,1)} %shard_map.55) | data formatting | bytes 1048576
where the time goes:
time: 159 us; the launch traced here: 158 us
  Pallas kernels  156 us (98%)
  local copies, waits for them, and re-layouts  1.88 us (1%)
    pallas_call x1, Pallas kernels, per_device(): pl.pallas_call(functools.partial(kernel, NX, NY, NZ), out_shape=jax.Shape...  156 us

commit v1 on v0

v1 whole, which is shorter than its diff:
```python
import functools

import jax
import jax.numpy as jnp
from jax import lax
from jax.experimental import pallas as pl
from jax.experimental.pallas import tpu as pltpu
from jax.sharding import PartitionSpec as P

NORM_EPS = 1e-06
MESH = pl.DeviceIdType.MESH
TS = 2


def kernel(NX, NY, NZ, EARLY, tok, gain_in, w_e, w_r, gain_out, out,
           TG, N, WE, WR, H, O, PR, RX,
           t_ls, t_ps, t_r, e_a, e_b, e_c, e_l, e_r, r_a, r_b, r_c, r_l, r_r, p_s, p_r, c_s, c_r):
    R, D = tok.shape
    DK, F = w_e.shape
    H4 = F // NZ
    RT = R // TS
    fs, tp = lax.axis_index("fs"), lax.axis_index("tp")
    z, y = fs // NY, fs % NY
    x, c = tp // 2, tp % 2
    pc = 1 - c
    peer = (fs, x * 2 + pc)

    def zdev(q):
        return (q * NY + y, tp)

    xs = [(x + j) % NX for j in range(1, NX)]
    ys = [(y + j) % NY for j in range(1, NY)]
    xdevs = [(fs, q * 2 + c) for q in xs]
    ydevs = [(z * NY + q, tp) for q in ys]

    barrier = pltpu.get_barrier_semaphore()
    others = [zdev((z + j) % NZ) for j in range(1, NZ)] + xdevs + ydevs + [peer]
    for dev in others:
        pl.semaphore_signal(barrier, inc=1, device_id=dev, device_id_type=MESH)
    pl.semaphore_wait(barrier, len(others))

    def rc(src, dst, ss, rs, dev):
        return pltpu.make_async_remote_copy(src_ref=src, dst_ref=dst, send_sem=ss, recv_sem=rs,
                                            device_id=dev, device_id_type=MESH)

    def guarded(cond, fn):
        if cond is None:
            fn()
        else:
            pl.when(cond)(fn)

    def landed(ref, sem):
        pltpu.make_async_copy(ref, ref, sem).wait()

    def at_distance(d):
        if d == 0:
            return [(z, 0, None)]
        return [(z - d, -1, z - d >= 0), (z + d, 1, z + d < NZ)]

    def rows_of(start, size, half):
        if half is None:
            return pl.ds(pl.multiple_of(start, size), size)
        return pl.ds(pl.multiple_of(start + half * (size // 2), size // 2), size // 2)

    def e_view(xq, zq, yq, half=None):
        return WE.at[xq, rows_of((zq * NY + yq) * DK, DK, half)]

    def r_view(xq, zq, yq, half=None):
        return WR.at[zq * NY + yq, rows_of(xq * H4, H4, half)]

    def e_piece(q):
        return w_e.at[:, pl.ds(pl.multiple_of(q * H4, H4), H4)]

    def r_piece(q):
        return w_r.at[pl.ds(pl.multiple_of(q * H4, H4), H4)]

    class Weight:
        def __init__(self, view, piece, a, b, cc, l, r):
            self.view, self.piece, self.a, self.b, self.c, self.l, self.r = view, piece, a, b, cc, l, r

    E = Weight(e_view, e_piece, e_a, e_b, e_c, e_l, e_r)
    W = Weight(r_view, r_piece, r_a, r_b, r_c, r_l, r_r)
    ways = ((xdevs, xs, ydevs, ys), (ydevs, ys, xdevs, xs))

    def along_line(w, d):
        for q, s, ok in at_distance(d):
            guarded(ok, lambda q=q: rc(w.piece(q), w.view(x, z, y), w.a.at[q], w.l.at[z], zdev(q)).start())

    def first(w, q):
        landed(w.view(x, q, y), w.l.at[q])
        for h in (0, 1):
            for j, dev in enumerate(ways[h][0]):
                rc(w.view(x, q, y, h), w.view(x, q, y, h), w.b.at[q, j, h], w.r.at[x, q, y, h], dev).start()
        for h in (0, 1):
            for j, dev in enumerate(ways[h][2]):
                rc(w.view(x, q, y, h), w.view(x, q, y, h), w.c.at[q, 0, j, h], w.r.at[x, q, y, h], dev).start()

    def second(w, q):
        for h in (0, 1):
            for i, m in enumerate(ways[h][1]):
                where = (m, q, y) if h == 0 else (x, q, m)
                landed(w.view(*where, h), w.r.at[(*where, h)])
                for j, dev in enumerate(ways[h][2]):
                    rc(w.view(*where, h), w.view(*where, h), w.c.at[q, 1 + i, j, h], w.r.at[(*where, h)], dev).start()

    def last(w, q):
        for h in (0, 1):
            for a in [x] + xs if h == 0 else xs:
                for b in ys if h == 0 else [y] + ys:
                    landed(w.view(a, q, b, h), w.r.at[a, q, b, h])

    def both(fn, w, d):
        for q, s, ok in at_distance(d):
            guarded(ok, lambda q=q: fn(w, q))

    def drain_weight(w):
        def body(q, carry):
            pl.when(q != z)(lambda: rc(w.piece(q), w.view(x, z, y), w.a.at[q], w.l.at[z], peer).wait_send())
            for h in (0, 1):
                v = w.view(x, q, y, h)
                for j in range(len(ways[h][0])):
                    rc(v, v, w.b.at[q, j, h], w.r.at[x, q, y, h], peer).wait_send()
                for i in range(1 + len(ways[h][1])):
                    for j in range(len(ways[h][2])):
                        rc(v, v, w.c.at[q, i, j, h], w.r.at[x, q, y, h], peer).wait_send()
            return carry

        lax.fori_loop(0, NZ, body, 0)

    def t_view(q, cc, u):
        return TG.at[q, cc, pl.ds(u * RT, RT)]

    def send_tokens(src, q, u, n, side, ok):
        guarded(ok, lambda: rc(src, t_view(q, c, u), t_ls.at[q, side, u], t_r.at[q, c, u], zdev(n)).start())

    def peer_tokens(src, q, u, ok):
        guarded(ok, lambda: rc(src, t_view(q, c, u), t_ps.at[q, u], t_r.at[q, c, u], peer).start())

    def tokens_step(d):
        for u in range(TS):
            for q, s, ok in at_distance(d):
                guarded(ok, lambda q=q, u=u: landed(t_view(q, c, u), t_r.at[q, c, u]))
                n = z - s
                send_tokens(t_view(q, c, u), q, u, n, (1 - s) // 2,
                            jnp.logical_and(ok, jnp.logical_and(n >= 0, n < NZ)))
                peer_tokens(t_view(q, c, u), q, u, ok)

    M = 2 * R
    sub = 32

    def norm_rows(q):
        for u in range(TS):
            landed(t_view(q, pc, u), t_r.at[q, pc, u])
        base = q * M if EARLY else 0

        def norm(i, carry):
            v = TG[q, i // (R // sub), pl.ds(pl.multiple_of((i % (R // sub)) * sub, sub), sub)].astype(jnp.float32)
            v = v * lax.rsqrt(jnp.mean(v * v, axis=-1, keepdims=True) + NORM_EPS) * gain_in[...]
            N[pl.ds(pl.multiple_of(base + i * sub, sub), sub)] = v.astype(jnp.bfloat16)
            return carry

        lax.fori_loop(0, M // sub, norm, 0)

    def expand_rows(q, carry):
        if not EARLY:
            norm_rows(q)
        rows = pl.ds(pl.multiple_of(q * M, M), M)
        src = rows if EARLY else slice(None)
        for i in range(NX):
            p = jnp.dot(N[src], WE[i], preferred_element_type=jnp.float32)
            H[rows, i * H4:(i + 1) * H4] = jnp.square(jnp.maximum(p, 0.0)).astype(jnp.bfloat16)
        return carry

    def norm_at(d):
        if EARLY:
            for q, s, ok in at_distance(d):
                guarded(ok, lambda q=q: norm_rows(q))

    big = 2 * M if NZ % 2 == 0 else M
    nb = NZ * M // big

    def columns(g):
        def body(k, carry):
            f, i = g * NY + k // nb, k % nb
            p = jnp.dot(H[pl.ds(pl.multiple_of(i * big, big), big)], WR[f], preferred_element_type=jnp.float32)
            O[pl.ds(i * (big // M), big // M), :, f] = p.astype(jnp.bfloat16).reshape(big // M, 2, R, DK)
            return carry

        lax.fori_loop(0, NY * nb, body, 0)

    def part(g):
        return pl.ds(g * NY, NY)

    def pair_copy(g):
        return rc(O.at[:, pc, part(g)], PR.at[:, part(g)], p_s.at[g], p_r.at[g], peer)

    def pass_on(q, g, slot, n):
        return rc(O.at[q, c, part(g)], RX.at[slot, part(g)], c_s.at[q, g], c_r.at[slot, g], zdev(n))

    def add_part(q, g, slots):
        for slot in slots:
            landed(RX.at[slot, part(g)], c_r.at[slot, g])

        def body(f, carry):
            s = O[q, c, f].astype(jnp.float32) + PR[q, f].astype(jnp.float32)
            for slot in slots:
                s += RX[slot, f].astype(jnp.float32)
            O[q, c, f] = s.astype(jnp.bfloat16)
            return carry

        lax.fori_loop(g * NY, (g + 1) * NY, body, 0)

    def flow(g, right):
        for j in range(NZ - 1):
            q = NZ - 1 - j if right else j
            n = z + 1 if right else z - 1
            ok = q > z if right else q < z
            has = z > 0 if right else z < NZ - 1
            slot = jnp.where(q == n, NZ, q) if right else q

            def step(q=q, n=n, slot=slot, has=has):
                pl.when(has)(lambda: add_part(q, g, [q]))
                pl.when(jnp.logical_not(has))(lambda: add_part(q, g, []))
                pass_on(q, g, slot, n).start()

            pl.when(ok)(step)

    def column_block(g):
        last(W, g)
        columns(g)
        pair_copy(g).start()

    def pair_in(g):
        landed(PR.at[:, part(g)], p_r.at[g])

    def stage(t):
        if t < NZ:
            for q, s, ok in at_distance(t):
                guarded(ok, lambda q=q: column_block(q))
        if 1 <= t <= NZ:
            for q, s, ok in at_distance(t - 1):
                guarded(ok, lambda q=q: pair_in(q))
        for right, hops in ((True, z), (False, NZ - 1 - z)):
            k = t - 1 - hops
            g = k if right else NZ - 1 - k
            pl.when(jnp.logical_and(k >= 0, k < NZ))(lambda g=g, right=right: flow(g, right))
        if t + 1 < NZ:
            both(second, W, t + 1)
        if t + 2 < NZ:
            both(first, W, t + 2)

    own = [pltpu.make_async_copy(t_src, t_view(z, c, u), t_r.at[z, c, u])
           for u, t_src in ((u, tok.at[pl.ds(u * RT, RT)]) for u in range(TS))]
    own += [pltpu.make_async_copy(E.piece(z), E.view(x, z, y), E.l.at[z]),
            pltpu.make_async_copy(W.piece(z), W.view(x, z, y), W.l.at[z])]
    for copy in own:
        copy.start()
    for u in range(TS):
        src = tok.at[pl.ds(u * RT, RT)]
        send_tokens(src, z, u, z - 1, 0, z >= 1)
        send_tokens(src, z, u, z + 1, 1, z + 1 < NZ)
        peer_tokens(src, z, u, None)
    along_line(E, 1)
    first(E, z)
    for d in range(2, NZ):
        along_line(E, d)
    first(W, z)
    second(E, z)
    for u in range(TS):
        landed(t_view(z, c, u), t_r.at[z, c, u])
    norm_at(0)
    tokens_step(1)
    second(W, z)
    both(first, E, 1)
    both(second, E, 1)
    for d in range(2, NZ):
        tokens_step(d)
        both(first, E, d)
        norm_at(d - 1)
        both(second, E, d)
    for d in range(1, NZ):
        along_line(W, d)
    norm_at(NZ - 1)
    for d in range(NZ):
        both(last, E, d)
    lax.fori_loop(0, NZ, expand_rows, 0)
    if NZ > 1:
        both(first, W, 1)
    for t in range(2 * NZ):
        stage(t)

    def finish(g, carry):
        pl.when(jnp.logical_and(z > 0, z < NZ - 1))(lambda: add_part(z, g, [z, NZ]))
        pl.when(z == 0)(lambda: add_part(z, g, [z]))
        pl.when(z == NZ - 1)(lambda: add_part(z, g, [NZ]))
        return carry

    lax.fori_loop(0, NZ, finish, 0)

    def squares(f, acc):
        m = O[z, c, f].astype(jnp.float32)
        return acc + jnp.sum(m * m, axis=-1, keepdims=True)

    total = lax.fori_loop(0, NZ * NY, squares, jnp.zeros((R, 1), jnp.float32))
    scale = lax.rsqrt(total / D + NORM_EPS)
    for f in range(NZ * NY):
        cols = slice(f * DK, (f + 1) * DK)
        out[:, cols] = (O[z, c, f].astype(jnp.float32) * scale * gain_out[:, cols]).astype(jnp.bfloat16)

    drain_weight(E)
    drain_weight(W)

    def drain(q, carry):
        for u in range(TS):
            v = t_view(q, c, u)
            rc(v, v, t_ps.at[q, u], t_r.at[q, c, u], peer).wait_send()
            pl.when(jnp.logical_and(q >= z, z >= 1))(
                lambda: rc(v, v, t_ls.at[q, 0, u], t_r.at[q, c, u], peer).wait_send())
            pl.when(jnp.logical_and(q <= z, z < NZ - 1))(
                lambda: rc(v, v, t_ls.at[q, 1, u], t_r.at[q, c, u], peer).wait_send())
        pair_copy(q).wait_send()
        for g in range(NZ):
            pl.when(q != z)(lambda: pass_on(q, g, q, z).wait_send())
        return carry

    lax.fori_loop(0, NZ, drain, 0)


def per_device(FS, TP, tokens, pre_gain, w_expand, w_reduce, post_gain):
    NX = TP // 2
    NY = max(k for k in range(1, FS + 1) if FS % k == 0 and (k == 1 or 2 * k * k <= FS))
    NZ = FS // NY
    R, D = tokens.shape
    DK, F = w_expand.shape
    H4 = F // NZ
    bf = jnp.bfloat16
    dma = pltpu.SemaphoreType.DMA
    mx = max(NX, NY)
    early = 2 * NZ * R * D * 2 <= 8 * 1024 * 1024
    vmem = pl.BlockSpec(memory_space=pltpu.VMEM)
    hbm = pl.BlockSpec(memory_space=pl.ANY)
    return pl.pallas_call(
        functools.partial(kernel, NX, NY, NZ, early),
        out_shape=jax.ShapeDtypeStruct((R, D), bf),
        in_specs=[hbm, vmem, hbm, hbm, vmem],
        out_specs=vmem,
        scratch_shapes=[
            pltpu.VMEM((NZ, 2, R, D), bf),
            pltpu.VMEM(((NZ if early else 1) * 2 * R, D), bf),
            pltpu.VMEM((NX, D, H4), bf),
            pltpu.VMEM((FS, NX * H4, DK), bf),
            pltpu.VMEM((NZ * 2 * R, NX * H4), bf),
            pltpu.VMEM((NZ, 2, FS, R, DK), bf),
            pltpu.VMEM((NZ, FS, R, DK), bf),
            pltpu.VMEM((NZ + 1, FS, R, DK), bf),
            dma((NZ, 2, TS)), dma((NZ, TS)), dma((NZ, 2, TS)),
            dma((NZ,)), dma((NZ, mx, 2)), dma((NZ, mx, mx, 2)), dma((NZ,)), dma((NX, NZ, NY, 2)),
            dma((NZ,)), dma((NZ, mx, 2)), dma((NZ, mx, mx, 2)), dma((NZ,)), dma((NX, NZ, NY, 2)),
            dma((NZ,)), dma((NZ,)), dma((NZ, NZ)), dma((NZ + 1, NZ)),
        ],
        compiler_params=pltpu.CompilerParams(
            collective_id=0, has_side_effects=True, vmem_limit_bytes=64 * 1024 * 1024 - 128 * 1024),
    )(tokens, pre_gain.reshape(1, D), w_expand, w_reduce, post_gain.reshape(1, D))


def solution(mesh):
    return jax.shard_map(
        functools.partial(per_device, mesh.shape["fs"], mesh.shape["tp"]),
        mesh=mesh,
        in_specs=(P(("fs", "tp"), None), P(), P("fs", "tp"), P("tp", "fs"), P()),
        out_specs=P(("fs", "tp"), None),
        check_vma=False,
    )
```

time: 159 us -> 132 us (0.83)
  the two profiles are of different devices: /device:TPU:20 before, /device:TPU:0 now
where the time goes in v1:
time: 132 us
  Pallas kernels  130 us (98%)
  local copies, waits for them, and re-layouts  1.88 us (1%)
    pallas_call x1, Pallas kernels, per_device(): pl.pallas_call(functools.partial(kernel, NX, NY, NZ, early), out_shape=ja...  130 us

profile of v1, /device:TPU:0, one launch (start us, length us, event | category | flops | bytes accessed | tf_op | source)
XLA Modules:
  0.0 132.1 jit_solution(4090990424438914393)
XLA Ops:
  0.0 130.2 %shard_map.55 = bf16[128,2048]{1,0:T(8,128)(2,1)} custom-call(bf16[128,2048]{1,0:T(8,128)(2,1)} %tok.1, f32[1,2048]{1,0:T(1,128)} %bitcast.2, bf16[256,2048]{1,0:T(8,128)(2,1)} %w_e.1, bf16[2048,256]{1,0:T(8,128)(2,1)} %w_r.1, f32[1,2048]{1,0:T(1,128)} %bitcast.3), custom_call_target="tpu_custom_call" | custom-call | tf_op jit(solution)/shard_map/pallas_call | solution.py:342
  130.2 1.9 %copy.7 = bf16[128,2048]{1,0:T(8,128)(2,1)} copy(bf16[128,2048]{1,0:T(8,128)(2,1)} %shard_map.55) | data formatting | bytes 1048576

commit v2 on v1

v2 whole, which is shorter than its diff:
```python
import functools

import jax
import jax.numpy as jnp
from jax import lax
from jax.experimental import pallas as pl
from jax.experimental.pallas import tpu as pltpu
from jax.sharding import PartitionSpec as P

NORM_EPS = 1e-06
MESH = pl.DeviceIdType.MESH
TS = 2


def kernel(NX, NY, NZ, EARLY, tok, gain_in, w_e, w_r, gain_out, out,
           TG, N, WE, WR, XE, XR, H, O, PR, RX,
           t_ls, t_ps, t_r, e_a, e_b, e_c, e_l, e_r, e_x, e_y, r_a, r_b, r_c, r_l, r_r, r_x, r_y, p_s, p_r, c_s, c_r):
    R, D = tok.shape
    DK, F = w_e.shape
    H4 = F // NZ
    RT = R // TS
    fs, tp = lax.axis_index("fs"), lax.axis_index("tp")
    z, y = fs // NY, fs % NY
    x, c = tp // 2, tp % 2
    pc = 1 - c
    peer = (fs, x * 2 + pc)

    low = 2 * z < NZ
    mz = jnp.where(low, z, NZ - 1 - z)
    toward = jnp.where(low, 1, -1)
    lifts = c == jnp.where(low, 1, 0)

    def src(m):
        return jnp.where(low, m, NZ - 1 - m)

    def zdev(q):
        return (q * NY + y, tp)

    xs = [(x + j) % NX for j in range(1, NX)]
    ys = [(y + j) % NY for j in range(1, NY)]
    xdevs = [(fs, q * 2 + c) for q in xs]
    ydevs = [(z * NY + q, tp) for q in ys]

    barrier = pltpu.get_barrier_semaphore()
    others = [zdev((z + j) % NZ) for j in range(1, NZ)] + xdevs + ydevs + [peer]
    for dev in others:
        pl.semaphore_signal(barrier, inc=1, device_id=dev, device_id_type=MESH)
    pl.semaphore_wait(barrier, len(others))

    def rc(src, dst, ss, rs, dev):
        return pltpu.make_async_remote_copy(src_ref=src, dst_ref=dst, send_sem=ss, recv_sem=rs,
                                            device_id=dev, device_id_type=MESH)

    def landed(ref, sem):
        pltpu.make_async_copy(ref, ref, sem).wait()

    def rows_of(start, size, half):
        if half is None:
            return pl.ds(pl.multiple_of(start, size), size)
        return pl.ds(pl.multiple_of(start + half * (size // 2), size // 2), size // 2)

    def e_view(xq, zq, yq, half=None):
        return WE.at[xq, rows_of((zq * NY + yq) * DK, DK, half)]

    def r_view(xq, zq, yq, half=None):
        return WR.at[zq * NY + yq, rows_of(xq * H4, H4, half)]

    def e_piece(q, half=None):
        cols = pl.ds(pl.multiple_of(q * H4, H4), H4)
        return w_e.at[:, cols] if half is None else w_e.at[rows_of(0, DK, half), cols]

    def r_piece(q, half=None):
        return w_r.at[rows_of(q * H4, H4, half)]

    class Weight:
        def __init__(self, view, piece, held, a, b, cc, l, r, sx, rx):
            self.view, self.piece, self.held, self.a, self.b, self.c = view, piece, held, a, b, cc
            self.l, self.r, self.sx, self.rx = l, r, sx, rx

    E = Weight(e_view, e_piece, XE, e_a, e_b, e_c, e_l, e_r, e_x, e_y)
    W = Weight(r_view, r_piece, XR, r_a, r_b, r_c, r_l, r_r, r_x, r_y)
    ways = ((xdevs, xs, ydevs, ys), (ydevs, ys, xdevs, xs))

    def hand_over(w, q):
        rc(w.piece(q), w.held.at[q], w.a.at[q], w.rx.at[q], peer).start()

    def along_line(w, q):
        rc(w.piece(q), w.view(x, z, y), w.a.at[q], w.l.at[z], zdev(q)).start()
        landed(w.held.at[q], w.rx.at[q])
        rc(w.held.at[q], w.view(x, z, y), w.sx.at[q], w.l.at[z], (q * NY + y, x * 2 + pc)).start()

    def first(w, q, own=False):
        if not own:
            landed(w.view(x, q, y), w.l.at[q])
        for h in (0, 1):
            for j, dev in enumerate(ways[h][0]):
                rc(w.piece(q, h) if own else w.view(x, q, y, h), w.view(x, q, y, h), w.b.at[q, j, h],
                   w.r.at[x, q, y, h], dev).start()
        for h in (0, 1):
            for j, dev in enumerate(ways[h][2]):
                rc(w.piece(q, h) if own else w.view(x, q, y, h), w.view(x, q, y, h), w.c.at[q, 0, j, h],
                   w.r.at[x, q, y, h], dev).start()

    def second(w, q):
        for h in (0, 1):
            for i, m in enumerate(ways[h][1]):
                where = (m, q, y) if h == 0 else (x, q, m)
                landed(w.view(*where, h), w.r.at[(*where, h)])
                for j, dev in enumerate(ways[h][2]):
                    rc(w.view(*where, h), w.view(*where, h), w.c.at[q, 1 + i, j, h], w.r.at[(*where, h)], dev).start()

    def last(w, q):
        for h in (0, 1):
            for a in [x] + xs if h == 0 else xs:
                for b in ys if h == 0 else [y] + ys:
                    landed(w.view(a, q, b, h), w.r.at[a, q, b, h])

    def drain_weight(w):
        def body(q, carry):
            pl.when(q != z)(lambda: rc(w.piece(q), w.view(x, z, y), w.a.at[q], w.l.at[z], peer).wait_send())
            pl.when(jnp.where(lifts, src(q) > mz, src(q) < mz))(
                lambda: rc(w.held.at[q], w.view(x, z, y), w.sx.at[q], w.l.at[z], peer).wait_send())
            for h in (0, 1):
                v = w.view(x, q, y, h)
                for j in range(len(ways[h][0])):
                    rc(v, v, w.b.at[q, j, h], w.r.at[x, q, y, h], peer).wait_send()
                for i in range(1 + len(ways[h][1])):
                    for j in range(len(ways[h][2])):
                        rc(v, v, w.c.at[q, i, j, h], w.r.at[x, q, y, h], peer).wait_send()
            return carry

        lax.fori_loop(0, NZ, body, 0)

    def t_view(q, cc, u):
        return TG.at[q, cc, pl.ds(u * RT, RT)]

    def send_tokens(source, q, cc, u, up):
        n = z + toward if up else z - toward
        dev = (n * NY + y, tp)
        rc(source, t_view(q, cc, u), t_ls.at[q, cc, u], t_r.at[q, cc, u], dev).start()

    def peer_tokens(source, q, cc, u):
        rc(source, t_view(q, cc, u), t_ps.at[q, cc, u], t_r.at[q, cc, u], peer).start()

    def relay_tokens(k, m, up):
        q = src(m)
        for u in range(TS):
            for cc in (0, 1):
                v = t_view(q, cc, u)
                landed(v, t_r.at[q, cc, u])
                if up or k > 0:
                    send_tokens(v, q, cc, u, up)
                peer_tokens(v, q, cc, u)

    def own_tokens(k, up):
        for u in range(TS):
            peer_tokens(tok.at[pl.ds(u * RT, RT)], z, c, u)
        linked = NZ > 1 and (up or k > 0)
        if linked:
            for u in range(TS):
                send_tokens(tok.at[pl.ds(u * RT, RT)], z, c, u, up)
        for u in range(TS):
            landed(t_view(z, pc, u), t_r.at[z, pc, u])
            if linked:
                send_tokens(t_view(z, pc, u), z, pc, u, up)

    def take_tokens(q):
        for u in range(TS):
            for cc in (0, 1):
                landed(t_view(q, cc, u), t_r.at[q, cc, u])

    M = 2 * R
    sub = 32

    def norm_rows(q):
        base = q * M if EARLY else 0

        def norm(i, carry):
            v = TG[q, i // (R // sub), pl.ds(pl.multiple_of((i % (R // sub)) * sub, sub), sub)].astype(jnp.float32)
            v = v * lax.rsqrt(jnp.mean(v * v, axis=-1, keepdims=True) + NORM_EPS) * gain_in[...]
            N[pl.ds(pl.multiple_of(base + i * sub, sub), sub)] = v.astype(jnp.bfloat16)
            return carry

        lax.fori_loop(0, M // sub, norm, 0)

    def expand_rows(q):
        if not EARLY:
            norm_rows(q)
        rows = pl.ds(pl.multiple_of(q * M, M), M)
        src = rows if EARLY else slice(None)
        for i in range(NX):
            p = jnp.dot(N[src], WE[i], preferred_element_type=jnp.float32)
            H[rows, i * H4:(i + 1) * H4] = jnp.square(jnp.maximum(p, 0.0)).astype(jnp.bfloat16)

    big = 2 * M if NZ % 2 == 0 else M
    nb = NZ * M // big

    def columns(g):
        def body(k, carry):
            f, i = g * NY + k // nb, k % nb
            p = jnp.dot(H[pl.ds(pl.multiple_of(i * big, big), big)], WR[f], preferred_element_type=jnp.float32)
            O[pl.ds(i * (big // M), big // M), :, f] = p.astype(jnp.bfloat16).reshape(big // M, 2, R, DK)
            return carry

        lax.fori_loop(0, NY * nb, body, 0)

    def part(g):
        return pl.ds(g * NY, NY)

    def pair_copy(q, g):
        return rc(O.at[q, pc, part(g)], PR.at[q, part(g)], p_s.at[g, q], p_r.at[g, q], peer)

    def pass_on(q, g, slot, n):
        return rc(O.at[q, c, part(g)], RX.at[slot, part(g)], c_s.at[q, g], c_r.at[slot, g], zdev(n))

    def add_part(q, g, slots):
        landed(PR.at[q, part(g)], p_r.at[g, q])
        for slot in slots:
            landed(RX.at[slot, part(g)], c_r.at[slot, g])

        def body(f, carry):
            s = O[q, c, f].astype(jnp.float32) + PR[q, f].astype(jnp.float32)
            for slot in slots:
                s += RX[slot, f].astype(jnp.float32)
            O[q, c, f] = s.astype(jnp.bfloat16)
            return carry

        lax.fori_loop(g * NY, (g + 1) * NY, body, 0)

    def unit(q, g, up, has):
        n = z + toward if up else z - toward
        slot = jnp.where(jnp.logical_and(q == n, low if up else jnp.logical_not(low)), NZ, q)
        add_part(q, g, [q] if has else [])
        pass_on(q, g, slot, n).start()

    def column_block(g):
        columns(g)
        lax.fori_loop(0, NZ, lambda q, carry: (pair_copy(q, g).start(), carry)[1], 0)

    def some_columns(q, g):
        def body(k, carry):
            f = g * NY + k
            p = jnp.dot(H[pl.ds(pl.multiple_of(q * M, M), M)], WR[f], preferred_element_type=jnp.float32)
            O[q, :, f] = p.astype(jnp.bfloat16).reshape(2, R, DK)
            return carry

        lax.fori_loop(0, NY, body, 0)
        pair_copy(q, g).start()

    def norm_own():
        for u in range(TS):
            landed(t_view(z, c, u), t_r.at[z, c, u])
        if EARLY:
            norm_rows(z)

    def token_time(k, m):
        d = abs(m - k)
        return 28 + 6 * (0 < k < m) if d == 1 else 22 + 12 * d + k

    def hidden_time(k, q):
        return 50.0 if q == k else max(41.5, token_time(k, q) + 2.5) + 1.5

    def first_w(k, m):
        d = abs(m - k)
        if d == 1:
            return 38 if m < k or k == 0 else 53
        return (60 if k == 0 else 62) + 6 * (d - 2)

    def second_w(k, m):
        d = abs(m - k)
        return (48.5 if m < k or k == 0 else 58) if d == 1 else first_w(k, m) + 6

    def columns_time(k, g):
        return (45.0 if k == 0 else 52.0) if g == k else second_w(k, g) + 5

    def unit_time(k, g, q):
        if k > 0:
            return unit_time(0, g, q) + 6 * k
        return max(columns_time(0, g), hidden_time(0, q)) + 3

    def program(k, up):
        ops = []

        def op(t, fn):
            ops.append((t, len(ops), fn))

        others = sorted((m for m in range(NZ) if m != k), key=lambda m: abs(m - k))
        op(0.2, lambda: first(E, z, True))
        op(0.3, lambda: own_tokens(k, up))
        op(5.5, lambda: second(E, z))
        op(6, norm_own)
        op(9 if k == 0 else 33, lambda: first(W, z, True))
        op(19 if k == 0 else 43.5, lambda: second(W, z))
        op(columns_time(k, k), lambda: landed(W.view(x, z, y), W.l.at[z]))
        op(columns_time(k, k), lambda: last(W, z))
        op(41, lambda: landed(E.view(x, z, y), E.l.at[z]))
        for m in range(NZ):
            op(41, lambda m=m: last(E, src(m)))
        for m in others:
            d, q = abs(m - k), src(m)
            mine = m > k if up else m < k
            if mine:
                op(0.22 + 0.01 * d, lambda q=q: along_line(E, q))
                sent = (37 if 0 < k < m else 0.4) if d == 1 else 45 + 0.1 * d
                op(sent, lambda q=q: along_line(W, q))
            else:
                op(0.1, lambda q=q: hand_over(E, q))
                op(0.15, lambda q=q: hand_over(W, q))
            t = token_time(k, m)
            comes = m < k if up else m > k
            if comes:
                op(t, lambda m=m: relay_tokens(k, m, up))
            else:
                op(t + 2.1, lambda q=q: take_tokens(q))
            if EARLY:
                op(t + 2.2, lambda q=q: norm_rows(q))
            e = 8.5 if d == 1 else 12 + 5 * d if k == 0 else 8.5 * d
            op(e, lambda q=q: first(E, q))
            op(min(33, e + (6.5 if k == 0 else 11.5)), lambda q=q: second(E, q))
            op(first_w(k, m), lambda q=q: first(W, q))
            op(second_w(k, m), lambda q=q: second(W, q))
            op(columns_time(k, m), lambda q=q: last(W, q))
        for m in range(NZ):
            op(hidden_time(k, m), lambda m=m: expand_rows(src(m)))
        latest = max(hidden_time(k, m) for m in range(NZ))
        ready = {}
        for g in range(NZ):
            if columns_time(k, g) >= latest:
                op(columns_time(k, g) + 0.1, lambda g=g: column_block(src(g)))
            for q in range(NZ - 1, -1, -1):
                ready[g, q] = max(columns_time(k, g), hidden_time(k, q)) + 0.1
                if columns_time(k, g) < latest:
                    op(ready[g, q], lambda g=g, q=q: some_columns(src(q), src(g)))
        for g in range(NZ):
            for q in range(NZ - 1, -1, -1):
                if q > k:
                    t = max(unit_time(k, g, q), ready[g, q] + 1)
                    op(t, lambda g=g, q=q: unit(src(q), src(g), True, k > 0))
                if q < k:
                    t = max(unit_time(NZ - 1 - k, NZ - 1 - g, NZ - 1 - q), ready[g, q] + 1)
                    op(t, lambda g=g, q=q: unit(src(q), src(g), False, True))
        for _, _, fn in sorted(ops, key=lambda o: o[:2]):
            fn()

    own = [pltpu.make_async_copy(t_src, t_view(z, c, u), t_r.at[z, c, u])
           for u, t_src in ((u, tok.at[pl.ds(u * RT, RT)]) for u in range(TS))]
    own += [pltpu.make_async_copy(E.piece(z), E.view(x, z, y), E.l.at[z]),
            pltpu.make_async_copy(W.piece(z), W.view(x, z, y), W.l.at[z])]
    for copy in own:
        copy.start()
    for k in range((NZ + 1) // 2):
        pl.when(jnp.logical_and(mz == k, lifts))(functools.partial(program, k, True))
        pl.when(jnp.logical_and(mz == k, jnp.logical_not(lifts)))(functools.partial(program, k, False))

    def finish(g, carry):
        pl.when(jnp.logical_and(z > 0, z < NZ - 1))(lambda: add_part(z, g, [z, NZ]))
        pl.when(z == 0)(lambda: add_part(z, g, [z]))
        pl.when(z == NZ - 1)(lambda: add_part(z, g, [NZ]))
        return carry

    lax.fori_loop(0, NZ, finish, 0)

    def squares(f, acc):
        m = O[z, c, f].astype(jnp.float32)
        return acc + jnp.sum(m * m, axis=-1, keepdims=True)

    total = lax.fori_loop(0, NZ * NY, squares, jnp.zeros((R, 1), jnp.float32))
    scale = lax.rsqrt(total / D + NORM_EPS)
    for f in range(NZ * NY):
        cols = slice(f * DK, (f + 1) * DK)
        out[:, cols] = (O[z, c, f].astype(jnp.float32) * scale * gain_out[:, cols]).astype(jnp.bfloat16)

    drain_weight(E)
    drain_weight(W)

    def drain(q, carry):
        m = src(q)
        for u in range(TS):
            for cc in (0, 1):
                v = t_view(q, cc, u)
                pl.when(jnp.where(q == z, c == cc, jnp.where(lifts, m < mz, m > mz)))(
                    lambda: rc(v, v, t_ps.at[q, cc, u], t_r.at[q, cc, u], peer).wait_send())
                pl.when(jnp.where(lifts, jnp.logical_and(m <= mz, NZ > 1), jnp.logical_and(m >= mz, mz > 0)))(
                    lambda: rc(v, v, t_ls.at[q, cc, u], t_r.at[q, cc, u], peer).wait_send())
        for g in range(NZ):
            pair_copy(q, g).wait_send()
            pl.when(q != z)(lambda: pass_on(q, g, q, z).wait_send())
        return carry

    lax.fori_loop(0, NZ, drain, 0)


def per_device(FS, TP, tokens, pre_gain, w_expand, w_reduce, post_gain):
    NX = TP // 2
    NY = max(k for k in range(1, FS + 1) if FS % k == 0 and (k == 1 or 2 * k * k <= FS))
    NZ = FS // NY
    R, D = tokens.shape
    DK, F = w_expand.shape
    H4 = F // NZ
    bf = jnp.bfloat16
    dma = pltpu.SemaphoreType.DMA
    mx = max(NX, NY)
    early = 2 * NZ * R * D * 2 <= 8 * 1024 * 1024
    vmem = pl.BlockSpec(memory_space=pltpu.VMEM)
    hbm = pl.BlockSpec(memory_space=pl.ANY)
    return pl.pallas_call(
        functools.partial(kernel, NX, NY, NZ, early),
        out_shape=jax.ShapeDtypeStruct((R, D), bf),
        in_specs=[hbm, vmem, hbm, hbm, vmem],
        out_specs=vmem,
        scratch_shapes=[
            pltpu.VMEM((NZ, 2, R, D), bf),
            pltpu.VMEM(((NZ if early else 1) * 2 * R, D), bf),
            pltpu.VMEM((NX, D, H4), bf),
            pltpu.VMEM((FS, NX * H4, DK), bf),
            pltpu.VMEM((NZ, DK, H4), bf),
            pltpu.VMEM((NZ, H4, DK), bf),
            pltpu.VMEM((NZ * 2 * R, NX * H4), bf),
            pltpu.VMEM((NZ, 2, FS, R, DK), bf),
            pltpu.VMEM((NZ, FS, R, DK), bf),
            pltpu.VMEM((NZ + 1, FS, R, DK), bf),
            dma((NZ, 2, TS)), dma((NZ, 2, TS)), dma((NZ, 2, TS)),
            dma((NZ,)), dma((NZ, mx, 2)), dma((NZ, mx, mx, 2)), dma((NZ,)), dma((NX, NZ, NY, 2)), dma((NZ,)), dma((NZ,)),
            dma((NZ,)), dma((NZ, mx, 2)), dma((NZ, mx, mx, 2)), dma((NZ,)), dma((NX, NZ, NY, 2)), dma((NZ,)), dma((NZ,)),
            dma((NZ, NZ)), dma((NZ, NZ)), dma((NZ, NZ)), dma((NZ + 1, NZ)),
        ],
        compiler_params=pltpu.CompilerParams(
            collective_id=0, has_side_effects=True, vmem_limit_bytes=64 * 1024 * 1024 - 128 * 1024),
    )(tokens, pre_gain.reshape(1, D), w_expand, w_reduce, post_gain.reshape(1, D))


def solution(mesh):
    return jax.shard_map(
        functools.partial(per_device, mesh.shape["fs"], mesh.shape["tp"]),
        mesh=mesh,
        in_specs=(P(("fs", "tp"), None), P(), P("fs", "tp"), P("tp", "fs"), P()),
        out_specs=P(("fs", "tp"), None),
        check_vma=False,
    )
```

time: 132 us -> 120 us (0.909)
  Pallas kernels: 130 us -> 118 us
    pallas_call x1, Pallas kernels: 130 us -> 118 us  [per_device(): pl.pallas_call(functools.partial(kernel, NX, NY, NZ, early), out_shape=ja...]
where the time goes in v2:
time: 120 us
  Pallas kernels  118 us (98%)
  local copies, waits for them, and re-layouts  1.88 us (2%)
    pallas_call x1, Pallas kernels, per_device(): pl.pallas_call(functools.partial(kernel, NX, NY, NZ, early), out_shape=ja...  118 us

profile of v2, /device:TPU:0, one launch (start us, length us, event | category | flops | bytes accessed | tf_op | source)
XLA Modules:
  0.0 120.1 jit_solution(9781375543054023910)
XLA Ops:
  0.0 118.2 %shard_map.55 = bf16[128,2048]{1,0:T(8,128)(2,1)} custom-call(bf16[128,2048]{1,0:T(8,128)(2,1)} %tok.1, f32[1,2048]{1,0:T(1,128)} %bitcast.2, bf16[256,2048]{1,0:T(8,128)(2,1)} %w_e.1, bf16[2048,256]{1,0:T(8,128)(2,1)} %w_r.1, f32[1,2048]{1,0:T(1,128)} %bitcast.3), custom_call_target="tpu_custom_call" | custom-call | tf_op jit(solution)/shard_map/pallas_call | solution.py:406
  118.2 1.9 %copy.7 = bf16[128,2048]{1,0:T(8,128)(2,1)} copy(bf16[128,2048]{1,0:T(8,128)(2,1)} %shard_map.55) | data formatting | bytes 1048576

commit v3 on v2

--- a/solution.py
+++ b/solution.py
@@ -192,18 +192,6 @@
             p = jnp.dot(N[src], WE[i], preferred_element_type=jnp.float32)
             H[rows, i * H4:(i + 1) * H4] = jnp.square(jnp.maximum(p, 0.0)).astype(jnp.bfloat16)
 
-    big = 2 * M if NZ % 2 == 0 else M
-    nb = NZ * M // big
-
-    def columns(g):
-        def body(k, carry):
-            f, i = g * NY + k // nb, k % nb
-            p = jnp.dot(H[pl.ds(pl.multiple_of(i * big, big), big)], WR[f], preferred_element_type=jnp.float32)
-            O[pl.ds(i * (big // M), big // M), :, f] = p.astype(jnp.bfloat16).reshape(big // M, 2, R, DK)
-            return carry
-
-        lax.fori_loop(0, NY * nb, body, 0)
-
     def part(g):
         return pl.ds(g * NY, NY)
 
@@ -233,10 +221,6 @@
         add_part(q, g, [q] if has else [])
         pass_on(q, g, slot, n).start()
 
-    def column_block(g):
-        columns(g)
-        lax.fori_loop(0, NZ, lambda q, carry: (pair_copy(q, g).start(), carry)[1], 0)
-
     def some_columns(q, g):
         def body(k, carry):
             f = g * NY + k
@@ -255,20 +239,22 @@
 
     def token_time(k, m):
         d = abs(m - k)
-        return 28 + 6 * (0 < k < m) if d == 1 else 22 + 12 * d + k
+        return 28 + 6 * (0 < k < m) if d == 1 else 26 + 11.5 * d + k
 
     def hidden_time(k, q):
         return 50.0 if q == k else max(41.5, token_time(k, q) + 2.5) + 1.5
 
     def first_w(k, m):
         d = abs(m - k)
-        if d == 1:
-            return 38 if m < k or k == 0 else 53
-        return (60 if k == 0 else 62) + 6 * (d - 2)
+        if k == 0:
+            return 38 if d == 1 else 56 + 13 * (d - 2)
+        return 38 if d == 1 and m < k else 56 if d == 1 else 61.8 + 10 * (d - 2)
 
     def second_w(k, m):
         d = abs(m - k)
-        return (48.5 if m < k or k == 0 else 58) if d == 1 else first_w(k, m) + 6
+        if k == 0:
+            return 46 if d == 1 else 61 + 13.5 * (d - 2)
+        return 47 if d == 1 and m < k else 62 if d == 1 else 66 + 10 * (d - 2)
 
     def columns_time(k, g):
         return (45.0 if k == 0 else 52.0) if g == k else second_w(k, g) + 5
@@ -301,7 +287,7 @@
             mine = m > k if up else m < k
             if mine:
                 op(0.22 + 0.01 * d, lambda q=q: along_line(E, q))
-                sent = (37 if 0 < k < m else 0.4) if d == 1 else 45 + 0.1 * d
+                sent = (37 if 0 < k < m else 0.4) if d == 1 else 36.9 if k > 0 else 52.9 - 0.1 * d
                 op(sent, lambda q=q: along_line(W, q))
             else:
                 op(0.1, lambda q=q: hand_over(E, q))
@@ -322,15 +308,11 @@
             op(columns_time(k, m), lambda q=q: last(W, q))
         for m in range(NZ):
             op(hidden_time(k, m), lambda m=m: expand_rows(src(m)))
-        latest = max(hidden_time(k, m) for m in range(NZ))
         ready = {}
         for g in range(NZ):
-            if columns_time(k, g) >= latest:
-                op(columns_time(k, g) + 0.1, lambda g=g: column_block(src(g)))
-            for q in range(NZ - 1, -1, -1):
+            for q in sorted(range(NZ), key=lambda q: -abs(q - k)):
                 ready[g, q] = max(columns_time(k, g), hidden_time(k, q)) + 0.1
-                if columns_time(k, g) < latest:
-                    op(ready[g, q], lambda g=g, q=q: some_columns(src(q), src(g)))
+                op(ready[g, q], lambda g=g, q=q: some_columns(src(q), src(g)))
         for g in range(NZ):
             for q in range(NZ - 1, -1, -1):
                 if q > k:
@@ -352,24 +334,6 @@
         pl.when(jnp.logical_and(mz == k, lifts))(functools.partial(program, k, True))
         pl.when(jnp.logical_and(mz == k, jnp.logical_not(lifts)))(functools.partial(program, k, False))
 
-    def finish(g, carry):
-        pl.when(jnp.logical_and(z > 0, z < NZ - 1))(lambda: add_part(z, g, [z, NZ]))
-        pl.when(z == 0)(lambda: add_part(z, g, [z]))
-        pl.when(z == NZ - 1)(lambda: add_part(z, g, [NZ]))
-        return carry
-
-    lax.fori_loop(0, NZ, finish, 0)
-
-    def squares(f, acc):
-        m = O[z, c, f].astype(jnp.float32)
-        return acc + jnp.sum(m * m, axis=-1, keepdims=True)
-
-    total = lax.fori_loop(0, NZ * NY, squares, jnp.zeros((R, 1), jnp.float32))
-    scale = lax.rsqrt(total / D + NORM_EPS)
-    for f in range(NZ * NY):
-        cols = slice(f * DK, (f + 1) * DK)
-        out[:, cols] = (O[z, c, f].astype(jnp.float32) * scale * gain_out[:, cols]).astype(jnp.bfloat16)
-
     drain_weight(E)
     drain_weight(W)
 
@@ -388,6 +352,29 @@
         return carry
 
     lax.fori_loop(0, NZ, drain, 0)
+
+    def finish(t, acc):
+        g = jnp.where(low, NZ - 1 - t, t)
+        landed(PR.at[z, part(g)], p_r.at[g, z])
+        pl.when(z > 0)(lambda: landed(RX.at[NZ, part(g)], c_r.at[NZ, g]))
+        pl.when(z < NZ - 1)(lambda: landed(RX.at[z, part(g)], c_r.at[z, g]))
+
+        def body(f, acc):
+            s = O[z, c, f].astype(jnp.float32) + PR[z, f].astype(jnp.float32)
+            s += jnp.where(z < NZ - 1, RX[z, f].astype(jnp.float32), 0.0)
+            s += jnp.where(z > 0, RX[NZ, f].astype(jnp.float32), 0.0)
+            O[z, c, f] = s.astype(jnp.bfloat16)
+            m = O[z, c, f].astype(jnp.float32)
+            return acc + m * m
+
+        return lax.fori_loop(g * NY, (g + 1) * NY, body, acc)
+
+    squares = lax.fori_loop(0, NZ, finish, jnp.zeros((R, DK), jnp.float32))
+    total = jnp.sum(squares, axis=-1, keepdims=True)
+    scale = lax.rsqrt(total / D + NORM_EPS)
+    for f in range(NZ * NY):
+        cols = slice(f * DK, (f + 1) * DK)
+        out[:, cols] = (O[z, c, f].astype(jnp.float32) * scale * gain_out[:, cols]).astype(jnp.bfloat16)
 
 
 def per_device(FS, TP, tokens, pre_gain, w_expand, w_reduce, post_gain):

time: 120 us -> 116 us (0.967); the launches traced: 120 us -> 115 us
  Pallas kernels: 118 us -> 113 us
    pallas_call x1, Pallas kernels: 118 us -> 113 us  [per_device(): pl.pallas_call(functools.partial(kernel, NX, NY, NZ, early), out_shape=ja...]
where the time goes in v3:
time: 116 us; the launch traced here: 115 us
  Pallas kernels  113 us (97%)
  local copies, waits for them, and re-layouts  1.88 us (2%)
    pallas_call x1, Pallas kernels, per_device(): pl.pallas_call(functools.partial(kernel, NX, NY, NZ, early), out_shape=ja...  113 us

profile of v3, /device:TPU:0, one launch (start us, length us, event | category | flops | bytes accessed | tf_op | source)
XLA Modules:
  0.0 114.8 jit_solution(17087496049551296273)
XLA Ops:
  0.0 112.9 %shard_map.55 = bf16[128,2048]{1,0:T(8,128)(2,1)} custom-call(bf16[128,2048]{1,0:T(8,128)(2,1)} %tok.1, f32[1,2048]{1,0:T(1,128)} %bitcast.2, bf16[256,2048]{1,0:T(8,128)(2,1)} %w_e.1, bf16[2048,256]{1,0:T(8,128)(2,1)} %w_r.1, f32[1,2048]{1,0:T(1,128)} %bitcast.3), custom_call_target="tpu_custom_call" | custom-call | tf_op jit(solution)/shard_map/pallas_call | solution.py:393
  112.9 1.9 %copy.7 = bf16[128,2048]{1,0:T(8,128)(2,1)} copy(bf16[128,2048]{1,0:T(8,128)(2,1)} %shard_map.55) | data formatting | bytes 1048576
